TPU v7x, 32 devices: a whole 2x2x4 slice. The times are simulated.
32 devices in a mesh: sp: 8 (over z, y), tp: 4 (over x, core).
Axes of the slice: x: 2, y: 2, z: 4, core: 2. Of those that a mesh axis runs over, the one named last changes fastest.
Arguments:
- queries: bfloat16 [8192, 1024], P('sp', 'tp'), may hold values from -300 to 300
- keys: bfloat16 [8192, 512], P('sp', 'tp'), may hold values from -6 to 6
- values: bfloat16 [8192, 512], P('sp', 'tp'), may hold values from -6 to 6
- sink_logits: float32 [16], P('tp'), may hold values from 1 to 6
- residual: bfloat16 [8192, 2048], P('sp'), may hold values from -3 to 3
- out_weight: bfloat16 [1024, 2048], P('tp'), may hold values from -0.5390625 to 0.5390625
- norm_gain: float32 [2048], replicated, may hold values from 0.1 to 1.9
- gate_weight: bfloat16 [2048, 5632], P('sp', 'tp'), may hold values from -0.125 to 0.125
- up_weight: bfloat16 [2048, 5632], P('sp', 'tp'), may hold values from -0.125 to 0.125
- down_weight: bfloat16 [2048, 5632], P('sp', 'tp'), may hold values from -0.1796875 to 0.1796875
Outputs:
- layer_out: bfloat16 [8192, 2048], P(('sp', 'tp'))
All inputs are finite; a program needn't handle non-finite values.
Results may differ from a plain program's by a relative error of at most 0.02.
Values may be sent and summed in bfloat16 or wider, within the bound.
No kernel may reach another device: no remote copies, remote signals or barrier semaphores. Data moves between devices by JAX's collectives and lax.ppermute only.
A program may use at most 64 MiB of HBM per device.

v0:
```python
import jax
import jax.numpy as jnp
from jax import lax
from jax.sharding import PartitionSpec as P

QH = 16
HD = 64
WINDOW = 128


def shifted(block, axis, distance):
    devices = range(lax.axis_size(axis))
    route = [(i - distance, i) for i in devices if i - distance in devices]
    return lax.ppermute(block, axis, route)


def attend(queries, keys, values, sink_logits):
    local_rows = queries.shape[0]
    kv_local = keys.shape[1] // HD
    heads_local = queries.shape[1] // HD
    groups = heads_local // kv_local
    blocks = local_rows // WINDOW
    key_value = jnp.concatenate([keys, values], axis=1)
    previous = shifted(key_value[local_rows - WINDOW :], "sp", 1)
    extended = jnp.concatenate([previous, key_value], axis=0)
    stacked = extended.reshape(blocks + 1, WINDOW, 2 * kv_local * HD)
    band = jnp.concatenate([stacked[:-1], stacked[1:]], axis=1)
    key_band = band[:, :, : kv_local * HD].reshape(blocks, 2 * WINDOW, kv_local, HD)
    value_band = band[:, :, kv_local * HD :].reshape(blocks, 2 * WINDOW, kv_local, HD)
    query_blocks = queries.reshape(blocks, WINDOW, kv_local, groups, HD)
    query_index = jnp.arange(WINDOW, dtype=jnp.int32)[:, None]
    key_index = jnp.arange(2 * WINDOW, dtype=jnp.int32)[None, :]
    distance = query_index - key_index + WINDOW
    offset = lax.axis_index("sp") * local_rows
    key_place = (
        offset
        + jnp.arange(blocks, dtype=jnp.int32)[:, None, None] * WINDOW
        + key_index[None]
        - WINDOW
    )
    valid = (distance >= 0) & (distance < WINDOW) & (key_place >= 0)
    head_number = (
        lax.axis_index("tp") * heads_local + jnp.arange(heads_local, dtype=jnp.int32) + 1
    ).astype(jnp.float32)
    slopes = (2.0 ** (-8.0 * head_number / QH)).reshape(kv_local, groups, 1, 1, 1)
    scores = jnp.einsum(
        "nqhgd,nkhd->hgnqk", query_blocks, key_band, preferred_element_type=jnp.float32
    ) * HD ** (-0.5)
    scores = scores - slopes * distance.astype(jnp.float32)
    scores = jnp.where(valid, scores, -jnp.inf)
    sinks = sink_logits.reshape(kv_local, groups, 1, 1, 1)
    top = jnp.maximum(jnp.max(scores, axis=-1, keepdims=True), sinks)
    expd = jnp.exp(scores - top)
    denom = jnp.sum(expd, axis=-1, keepdims=True) + jnp.exp(sinks - top)
    weights = (expd / denom).astype(jnp.bfloat16)
    output = jnp.einsum(
        "hgnqk,nkhd->nqhgd", weights, value_band, preferred_element_type=jnp.float32
    )
    return output.reshape(local_rows, heads_local * HD).astype(jnp.bfloat16)


def rms_scale(rows, norm_gain):
    rows_f = rows.astype(jnp.float32)
    scale = lax.rsqrt(jnp.mean(rows_f * rows_f, axis=-1, keepdims=True) + 1e-06)
    return (rows_f * scale * norm_gain).astype(jnp.bfloat16)


def expand_rows(normed, gate_full, up_full):
    gate = jnp.dot(normed, gate_full, preferred_element_type=jnp.float32)
    upper = jnp.dot(normed, up_full, preferred_element_type=jnp.float32)
    return (jax.nn.silu(gate) * upper).astype(jnp.bfloat16)


def per_device(
    queries,
    keys,
    values,
    sink_logits,
    residual,
    out_weight,
    norm_gain,
    gate_weight,
    up_weight,
    down_weight,
):
    attended = attend(queries, keys, values, sink_logits)
    local_rows = queries.shape[0]
    tp_count = lax.axis_size("tp")
    own_rows = local_rows // tp_count
    first_row = lax.axis_index("tp") * own_rows
    partial_sum = jnp.dot(attended, out_weight, preferred_element_type=jnp.float32)
    projected = lax.psum(partial_sum.astype(jnp.bfloat16), "tp").astype(jnp.float32)
    mixed_all = (residual.astype(jnp.float32) + projected).astype(jnp.bfloat16)
    mixed_rows = lax.dynamic_slice_in_dim(mixed_all, first_row, own_rows, 0)
    gate_full, up_full = (
        lax.all_gather(gate_weight, "sp", axis=0, tiled=True),
        lax.all_gather(up_weight, "sp", axis=0, tiled=True),
    )
    hidden = expand_rows(rms_scale(mixed_all, norm_gain), gate_full, up_full)
    down_full = lax.all_gather(down_weight, "sp", axis=0, tiled=True)
    expanded = lax.psum_scatter(
        lax.dot_general(
            hidden, down_full, (((1,), (1,)), ((), ())), preferred_element_type=jnp.float32
        ).astype(jnp.bfloat16),
        "tp",
        scatter_dimension=0,
        tiled=True,
    ).astype(jnp.float32)
    return (mixed_rows.astype(jnp.float32) + 0.5 * expanded).astype(jnp.bfloat16)


def solution(mesh):
    return jax.shard_map(
        per_device,
        mesh=mesh,
        in_specs=(
            P("sp", "tp"),
            P("sp", "tp"),
            P("sp", "tp"),
            P("tp"),
            P("sp", None),
            P("tp", None),
            P(),
            P("sp", "tp"),
            P("sp", "tp"),
            P("sp", "tp"),
        ),
        out_specs=P(("sp", "tp"), None),
        check_vma=False,
    )
```

profile of v0, /device:TPU:0, one launch (start us, length us, event | category | flops | bytes accessed | tf_op | source)
XLA Modules:
  0.0 386.4 jit_solution(11114447815396450490)
XLA Ops:
  7.4 1.1 constant_dynamic-update-slice_fusion.1
  8.5 1.0 constant_dynamic-update-slice_fusion
  9.5 4.9 %collective-permute-start = (bf16[128,256]{1,0:T(8,128)(2,1)S(1)}, bf16[128,256]{1,0:T(8,128)(2,1)S(1)}, u32[]{:S(2)}, u32[]{:S(2)}) collective-permute-start(bf16[128,256]{1,0:T(8,128)(2,1)S(1)} %slice.25), channel_id=1, source_target_pairs={{0,4},{4,8},{8,12},{12,16},{16,20},{20,24},{24,28},{1,5},{5,9},{9,... | collective-permute-start | bytes 196616 | tf_op jit(solution)/shard_map/ppermute | solution.py:14
  14.5 0.1 add_compare_fusion
  14.6 0.1 broadcast_multiply_fusion
  14.7 0.3 broadcast_and_fusion
  15.0 3.2 reshape.128
  18.3 0.7 max.18
  19.1 0.3 pad_maximum_fusion
  19.3 0.2 copy.21
  19.5 2.3 fusion.5
  21.9 0.1 broadcast_maximum_fusion
  22.0 1.9 copy-done.1
  23.8 1.1 fusion.4
  24.9 0.1 exponential_add_fusion
  25.0 0.2 copy.20
  25.3 3.5 fusion.11
  28.7 0.3 copy.26
  29.1 3.3 convolution_convert_fusion.1
  32.5 0.5 all-gather.4.cloned.1.call-update
  33.0 0.5 all-gather.6.cloned.1.call-update
  33.6 0.5 all-gather.8.cloned.1.call-update
  34.2 0.2 reduce-scatter.2.cloned.1.call-start
  34.4 83.9 %all-reduce.2.cloned.1.call-done = bf16[1024,2048]{1,0:T(8,128)(2,1)} async-done(((bf16[1024,2048]{1,0:T(8,128)(2,1)}), bf16[1024,2048]{1,0:T(8,128)(2,1)}) %all-reduce.2.cloned.1.call-update) | async-done | bytes 4194320 | tf_op jit(solution)/shard_map/psum | solution.py:92
  118.4 7.5 %fusion = (f32[1024]{0:T(1024)S(1)}, bf16[1024,2048]{1,0:T(8,128)(2,1)}) fusion(bf16[1024,2048]{1,0:T(8,128)(2,1)} %all-reduce.2.cloned.1.call-done, bf16[1024,2048]{1,0:T(8,128)(2,1)} %param.14), kind=kLoop, calls=%fused_computation.2 | loop fusion | flops 14679040 | bytes 12587008 | tf_op jit(solution)/shard_map/reduce_sum | solution.py:64
  125.8 1.7 all-gather.4.cloned.1.call-done
  127.5 11.9 %fusion.15 = f32[1024,1408]{1,0:T(8,128)} fusion(bf16[2048,1408]{1,0:T(8,128)(2,1)} %all-gather.4.cloned.1.call-done, bf16[1024,2048]{1,0:T(8,128)(2,1)} %get-tuple-element.6, f32[2048]{0:T(1024)S(1)} %copy-done.2, f32[1024]{0:T(1024)S(1)} %add_rsqrt_fusion), kind=kOutput, calls=%fused_computation.20 | convolution fusion | flops 5913968640 | bytes 15740928 | tf_op jit(solution)/shard_map/dot_general | solution.py:69
  139.5 80.4 %all-gather.6.cloned.1.call-done = bf16[2048,1408]{1,0:T(8,128)(2,1)} async-done(((bf16[256,1408]{1,0:T(8,128)(2,1)}), bf16[2048,1408]{1,0:T(8,128)(2,1)}) %all-gather.6.cloned.1.call-update) | async-done | bytes 5767184 | tf_op jit(solution)/shard_map/all_gather | solution.py:97
  219.9 92.4 %all-gather.8.cloned.1.call-done = bf16[2048,1408]{1,0:T(8,128)(2,1)} async-done(((bf16[256,1408]{1,0:T(8,128)(2,1)}), bf16[2048,1408]{1,0:T(8,128)(2,1)}) %all-gather.8.cloned.1.call-update) | async-done | bytes 5767184 | tf_op jit(solution)/shard_map/all_gather | solution.py:100
  312.2 20.8 %convolution_convert_fusion = bf16[1024,2048]{1,0:T(8,128)(2,1)} fusion(bf16[2048,1408]{1,0:T(8,128)(2,1)} %all-gather.8.cloned.1.call-done, f32[1024,1408]{1,0:T(8,128)} %fusion.15, bf16[2048,1408]{1,0:T(8,128)(2,1)} %all-gather.6.cloned.1.call-done, bf16[1024,2048]{1,0:T(8,128)(2,1)} %get-tuple-element.6, f32[2048]{0:T(1024)S(1)} %copy-done.2, ...), kind=kOutput, calls=%fused_computation.11 | convolution fusion | flops 11830296576 | bytes 25702400 | tf_op jit(solution)/shard_map/dot_general | solution.py:102
  333.1 42.8 %reduce-scatter.2.cloned.1.call-done = bf16[256,2048]{1,0:T(8,128)(2,1)} async-done(((bf16[1024,2048]{1,0:T(8,128)(2,1)}), bf16[256,2048]{1,0:T(8,128)(2,1)}) %reduce-scatter.2.cloned.1.call-update) | async-done | bytes 1048592 | tf_op jit(solution)/shard_map/reduce_scatter | solution.py:101
  375.9 2.9 add_convert_fusion.1
  (19 shorter events, 0.3 us)
Async XLA Ops:
  7.4 21.7 %copy-start = (bf16[256,2048]{1,0:T(8,128)(2,1)S(1)}, bf16[256,2048]{1,0:T(8,128)(2,1)}, u32[]{:S(2)}) copy-start(bf16[256,2048]{1,0:T(8,128)(2,1)} %param.15) | copy-start | bytes 3145732
  7.4 111.0 %all-reduce.2.cloned.1.call-start = ((), (), s32[]{:S(2)}) async-start(), calls=%async_computation.1 | async-start | bytes 8388608 | tf_op jit(solution)/shard_map/psum | solution.py:92
  9.5 9.5 %collective-permute-start = (bf16[128,256]{1,0:T(8,128)(2,1)S(1)}, bf16[128,256]{1,0:T(8,128)(2,1)S(1)}, u32[]{:S(2)}, u32[]{:S(2)}) collective-permute-start(bf16[128,256]{1,0:T(8,128)(2,1)S(1)} %slice.25), channel_id=1, source_target_pairs={{0,4},{4,8},{8,12},{12,16},{16,20},{20,24},{24,28},{1,5},{5,9},{9,... | collective-permute-start | bytes 196616 | tf_op jit(solution)/shard_map/ppermute | solution.py:14
  21.9 1.9 copy-start.1
  32.4 95.1 %all-gather.4.cloned.1.call-start = ((), (), s32[]{:S(2)}) async-start(), calls=%async_computation.2 | async-start | bytes 6488064 | tf_op jit(solution)/shard_map/all_gather | solution.py:96
  33.0 186.9 %all-gather.6.cloned.1.call-start = ((), (), s32[]{:S(2)}) async-start(), calls=%async_computation.3 | async-start | bytes 6488064 | tf_op jit(solution)/shard_map/all_gather | solution.py:97
  33.6 278.7 %all-gather.8.cloned.1.call-start = ((), (), s32[]{:S(2)}) async-start(), calls=%async_computation.4 | async-start | bytes 6488064 | tf_op jit(solution)/shard_map/all_gather | solution.py:100
  34.2 93.4 %copy-start.2 = (f32[2048]{0:T(1024)S(1)}, f32[2048]{0:T(1024)}, u32[]{:S(2)}) copy-start(f32[2048]{0:T(1024)} %param.16) | copy-start | bytes 24580
  34.2 341.8 %reduce-scatter.2.cloned.1.call-start = ((), (), s32[]{:S(2)}) async-start(), calls=%async_computation.5 | async-start | bytes 5242880 | tf_op jit(solution)/shard_map/reduce_scatter | solution.py:101
Sparse Core Ops, SparseCore 0:
  32.5 85.7 all-reduce.1
  333.2 42.6 reduce-scatter.1
Sparse Core Ops, SparseCore 1:
  35.1 92.4 all-gather.3
  129.6 90.2 all-gather.5
  222.0 90.2 all-gather.7
where the time goes:
time: 387 us; the launch traced here: 386 us
  waiting for transfers between devices  303 us (78%)
  matrix products  41.9 us (11%)
  between operations  15.2 us (4%)
  other arithmetic  12.5 us (3%)
  local copies, waits for them, and re-layouts  8.71 us (2%)
  starting transfers between devices  5.25 us (1%)
    all_gather x1, waiting for transfers between devices, per_device(): down_full = lax.all_gather(down_weight, 'sp', axis=0, tiled=True)  92.4 us
    psum x1, waiting for transfers between devices, per_device(): lax.psum(partial_sum.astype(jnp.bfloat16), 'tp').astype(jnp.float32)  83.9 us
    all_gather x1, waiting for transfers between devices, per_device(): lax.all_gather(up_weight, 'sp', axis=0, tiled=True)  80.4 us
    reduce_scatter x1, waiting for transfers between devices, per_device(): lax.psum_scatter(lax.dot_general(hidden, down_full, (((1,), (1,)), ((), (...  42.8 us
    dot_general x1, matrix products, per_device(): lax.dot_general(hidden, down_full, (((1,), (1,)), ((), ())), preferred_el...  20.8 us
    dot_general x1, matrix products, expand_rows(): gate = jnp.dot(normed, gate_full, preferred_element_type=jnp.float32)  11.9 us
  transfers between devices with their start and end apart: 6, of which 5 were waited for; matrix products, arithmetic and copies ran while one was open for 6% of the time, Pallas kernels for 0%

commit v1 on v0

--- a/solution.py
+++ b/solution.py
@@ -97,7 +97,13 @@
         lax.all_gather(up_weight, "sp", axis=0, tiled=True),
     )
     hidden = expand_rows(rms_scale(mixed_all, norm_gain), gate_full, up_full)
-    down_full = lax.all_gather(down_weight, "sp", axis=0, tiled=True)
+    n_dev = lax.axis_size("sp")
+    moving, shards = (down_weight, [down_weight])
+    for _ in range(n_dev - 1):
+        moving = lax.ppermute(moving, "sp", [(i_2, (i_2 + 1) % n_dev) for i_2 in range(n_dev)])
+        shards.insert(0, moving)
+    line = jnp.concatenate(shards, axis=0)
+    down_full = jnp.roll(line, (lax.axis_index("sp") + 1) * down_weight.shape[0], axis=0)
     expanded = lax.psum_scatter(
         lax.dot_general(
             hidden, down_full, (((1,), (1,)), ((), ())), preferred_element_type=jnp.float32

time: 387 us -> 366 us (0.946)
  waiting for transfers between devices: 303 us -> 262 us
  local copies, waits for them, and re-layouts: 8.71 us -> 29.3 us
    ppermute x0 -> x7, waiting for transfers between devices: none -> 200 us  [per_device(): lax.ppermute(moving, 'sp', [(i_2, (i_2 + 1) % n_dev) for i_2 in range(n_d...]
    all_gather x1 -> x0, waiting for transfers between devices: 92.4 us -> none  [per_device(): down_full = lax.all_gather(down_weight, 'sp', axis=0, tiled=True)]
    psum x1, waiting for transfers between devices: 83.9 us -> 0.01 us  [per_device(): lax.psum(partial_sum.astype(jnp.bfloat16), 'tp').astype(jnp.float32)]
    all_gather x1, waiting for transfers between devices: 80.4 us -> 18.3 us  [per_device(): lax.all_gather(up_weight, 'sp', axis=0, tiled=True)]
    unnamed x7 -> x28, local copies, waits for them, and re-layouts: 2.95 us -> 22.6 us
  transfers between devices with their start and end apart: 6 -> 12, of which waited for: 5 -> 9; matrix products, arithmetic and copies ran while one was open for 6% -> 12% of each run, Pallas kernels for 0% -> 0%
where the time goes in v1:
time: 366 us
  waiting for transfers between devices  262 us (72%)
  matrix products  39.8 us (11%)
  local copies, waits for them, and re-layouts  29.3 us (8%)
  between operations  15 us (4%)
  other arithmetic  12.6 us (3%)
  starting transfers between devices  7.53 us (2%)
    ppermute x7, waiting for transfers between devices, per_device(): lax.ppermute(moving, 'sp', [(i_2, (i_2 + 1) % n_dev) for i_2 in range(n_d...  200 us
    reduce_scatter x1, waiting for transfers between devices, per_device(): lax.psum_scatter(lax.dot_general(hidden, down_full, (((1,), (1,)), ((), (...  43.2 us
    unnamed x28, local copies, waits for them, and re-layouts  22.6 us
    dot_general x1, matrix products, per_device(): lax.dot_general(hidden, down_full, (((1,), (1,)), ((), ())), preferred_el...  20.9 us
    all_gather x1, waiting for transfers between devices, per_device(): lax.all_gather(up_weight, 'sp', axis=0, tiled=True)  18.3 us
    dot_general x1, matrix products, expand_rows(): gate = jnp.dot(normed, gate_full, preferred_element_type=jnp.float32)  11.9 us
    reduce_sum x1, other arithmetic, rms_scale(): scale = lax.rsqrt(jnp.mean(rows_f * rows_f, axis=-1, keepdims=True) + 1e-06)  7.52 us
  transfers between devices with their start and end apart: 12, of which 9 were waited for; matrix products, arithmetic and copies ran while one was open for 12% of the time, Pallas kernels for 0%

profile of v1, /device:TPU:0, one launch (start us, length us, event | category | flops | bytes accessed | tf_op | source)
XLA Modules:
  0.0 365.8 jit_solution(1417598632741641542)
XLA Ops:
  7.4 1.1 constant_dynamic-update-slice_fusion.1
  8.5 1.0 constant_dynamic-update-slice_fusion
  9.5 4.9 %collective-permute-start = (bf16[128,256]{1,0:T(8,128)(2,1)S(1)}, bf16[128,256]{1,0:T(8,128)(2,1)S(1)}, u32[]{:S(2)}, u32[]{:S(2)}) collective-permute-start(bf16[128,256]{1,0:T(8,128)(2,1)S(1)} %slice.25), channel_id=1, source_target_pairs={{0,4},{4,8},{8,12},{12,16},{16,20},{20,24},{24,28},{1,5},{5,9},{9,... | collective-permute-start | bytes 196616 | tf_op jit(solution)/shard_map/ppermute | solution.py:14
  15.0 3.2 reshape.128
  19.8 2.3 fusion.10
  22.2 1.1 fusion.9
  23.4 1.3 fusion.16
  25.0 3.3 convolution_convert_fusion
  29.0 1.6 collective-permute-start.1
  30.6 24.3 %collective-permute-done.1 = bf16[256,1408]{1,0:T(8,128)(2,1)S(1)} collective-permute-done((bf16[256,1408]{1,0:T(8,128)(2,1)S(1)}, bf16[256,1408]{1,0:T(8,128)(2,1)S(1)}, u32[]{:S(2)}, u32[]{:S(2)}) %collective-permute-start.1) | collective-permute-done | bytes 720928 | tf_op jit(solution)/shard_map/ppermute | solution.py:103
  55.9 32.2 %collective-permute-done.2 = bf16[256,1408]{1,0:T(8,128)(2,1)S(1)} collective-permute-done((bf16[256,1408]{1,0:T(8,128)(2,1)S(1)}, bf16[256,1408]{1,0:T(8,128)(2,1)S(1)}, u32[]{:S(2)}, u32[]{:S(2)}) %collective-permute-start.2) | collective-permute-done | bytes 720928 | tf_op jit(solution)/shard_map/ppermute | solution.py:103
  88.1 35.0 %collective-permute-done.3 = bf16[256,1408]{1,0:T(8,128)(2,1)S(1)} collective-permute-done((bf16[256,1408]{1,0:T(8,128)(2,1)S(1)}, bf16[256,1408]{1,0:T(8,128)(2,1)S(1)}, u32[]{:S(2)}, u32[]{:S(2)}) %collective-permute-start.3) | collective-permute-done | bytes 720928 | tf_op jit(solution)/shard_map/ppermute | solution.py:103
  123.0 35.1 %collective-permute-done.4 = bf16[256,1408]{1,0:T(8,128)(2,1)S(1)} collective-permute-done((bf16[256,1408]{1,0:T(8,128)(2,1)S(1)}, bf16[256,1408]{1,0:T(8,128)(2,1)S(1)}, u32[]{:S(2)}, u32[]{:S(2)}) %collective-permute-start.4) | collective-permute-done | bytes 720928 | tf_op jit(solution)/shard_map/ppermute | solution.py:103
  159.0 24.7 %collective-permute-done.5 = bf16[256,1408]{1,0:T(8,128)(2,1)} collective-permute-done((bf16[256,1408]{1,0:T(8,128)(2,1)S(1)}, bf16[256,1408]{1,0:T(8,128)(2,1)}, u32[]{:S(2)}, u32[]{:S(2)}) %collective-permute-start.5) | collective-permute-done | bytes 720928 | tf_op jit(solution)/shard_map/ppermute | solution.py:103
  183.7 32.8 %collective-permute-done.6 = bf16[256,1408]{1,0:T(8,128)(2,1)} collective-permute-done((bf16[256,1408]{1,0:T(8,128)(2,1)}, bf16[256,1408]{1,0:T(8,128)(2,1)}, u32[]{:S(2)}, u32[]{:S(2)}) %collective-permute-start.6) | collective-permute-done | bytes 720928 | tf_op jit(solution)/shard_map/ppermute | solution.py:103
  216.5 7.5 %fusion = (f32[1024]{0:T(1024)S(1)}, bf16[1024,2048]{1,0:T(8,128)(2,1)}) fusion(bf16[1024,2048]{1,0:T(8,128)(2,1)} %all-reduce.2.cloned.1.call-done, bf16[1024,2048]{1,0:T(8,128)(2,1)} %param.14), kind=kLoop, calls=%fused_computation.2 | loop fusion | flops 14679040 | bytes 12587008 | tf_op jit(solution)/shard_map/reduce_sum | solution.py:64
  224.0 15.5 %collective-permute-done.7 = bf16[256,1408]{1,0:T(8,128)(2,1)} collective-permute-done((bf16[256,1408]{1,0:T(8,128)(2,1)}, bf16[256,1408]{1,0:T(8,128)(2,1)}, u32[]{:S(2)}, u32[]{:S(2)}) %collective-permute-start.7) | collective-permute-done | bytes 720928 | tf_op jit(solution)/shard_map/ppermute | solution.py:103
  239.5 2.1 constant_dynamic-update-slice_fusion.17
  241.6 2.0 constant_dynamic-update-slice_fusion.16
  243.6 2.1 constant_dynamic-update-slice_fusion.15
  245.6 1.0 constant_dynamic-update-slice_fusion.14
  248.5 0.9 constant_dynamic-update-slice_fusion.11
  250.3 2.1 constant_dynamic-update-slice_fusion.9
  252.4 2.0 constant_dynamic-update-slice_fusion.8
  254.4 2.0 constant_dynamic-update-slice_fusion.7
  257.3 1.0 constant_dynamic-update-slice_fusion.5
  258.3 1.0 constant_dynamic-update-slice_fusion.4
  261.1 11.9 %fusion.20 = f32[1024,1408]{1,0:T(8,128)} fusion(bf16[2048,1408]{1,0:T(8,128)(2,1)} %all-gather.3.cloned.1.call-done, bf16[1024,2048]{1,0:T(8,128)(2,1)} %get-tuple-element.6, f32[2048]{0:T(1024)S(1)} %copy-done.5, f32[1024]{0:T(1024)S(1)} %add_rsqrt_fusion), kind=kOutput, calls=%fused_computation.22 | convolution fusion | flops 5913968640 | bytes 15740928 | tf_op jit(solution)/shard_map/dot_general | solution.py:69
  273.0 18.3 %all-gather.5.cloned.1.call-done = bf16[2048,1408]{1,0:T(8,128)(2,1)} async-done(((bf16[256,1408]{1,0:T(8,128)(2,1)}), bf16[2048,1408]{1,0:T(8,128)(2,1)}) %all-gather.5.cloned.1.call-update) | async-done | bytes 5767184 | tf_op jit(solution)/shard_map/all_gather | solution.py:97
  291.3 20.9 %fusion.6 = bf16[1024,2048]{1,0:T(8,128)(2,1)} fusion(bf16[4096,1408]{1,0:T(8,128)(2,1)} %constant_dynamic-update-slice_fusion.2, s32[]{:T(128)S(6)} %select_n.23, f32[1024,1408]{1,0:T(8,128)} %fusion.20, bf16[2048,1408]{1,0:T(8,128)(2,1)} %all-gather.5.cloned.1.call-done, bf16[1024,2048]{1,0:T(8,128)(2,1)} %get-tuple-element.6, f32[2048]{0:T(1024)S(1)} %copy-done.5, ...), kind=kOutput, calls=%fused_computation.13 | convolution fusion | flops 11830296576 | bytes 25702404 | tf_op jit(solution)/shard_map/dot_general | solution.py:108
  312.3 43.2 %reduce-scatter.2.cloned.1.call-done = bf16[256,2048]{1,0:T(8,128)(2,1)} async-done(((bf16[1024,2048]{1,0:T(8,128)(2,1)}), bf16[256,2048]{1,0:T(8,128)(2,1)}) %reduce-scatter.2.cloned.1.call-update) | async-done | bytes 1048592 | tf_op jit(solution)/shard_map/reduce_scatter | solution.py:107
  355.4 2.9 add_convert_fusion.1
  (52 shorter events, 10.6 us)
Async XLA Ops:
  7.4 17.6 %copy-start = (bf16[256,2048]{1,0:T(8,128)(2,1)S(1)}, bf16[256,2048]{1,0:T(8,128)(2,1)}, u32[]{:S(2)}) copy-start(bf16[256,2048]{1,0:T(8,128)(2,1)} %param.15) | copy-start | bytes 3145732
  7.4 209.1 %all-reduce.2.cloned.1.call-start = ((), (), s32[]{:S(2)}) async-start(), calls=%async_computation.1 | async-start | bytes 8388608 | tf_op jit(solution)/shard_map/psum | solution.py:92
  9.5 9.5 %collective-permute-start = (bf16[128,256]{1,0:T(8,128)(2,1)S(1)}, bf16[128,256]{1,0:T(8,128)(2,1)S(1)}, u32[]{:S(2)}, u32[]{:S(2)}) collective-permute-start(bf16[128,256]{1,0:T(8,128)(2,1)S(1)} %slice.25), channel_id=1, source_target_pairs={{0,4},{4,8},{8,12},{12,16},{16,20},{20,24},{24,28},{1,5},{5,9},{9,... | collective-permute-start | bytes 196616 | tf_op jit(solution)/shard_map/ppermute | solution.py:14
  25.0 4.0 %copy-start.2 = (bf16[256,1408]{1,0:T(8,128)(2,1)S(1)}, bf16[256,1408]{1,0:T(8,128)(2,1)}, u32[]{:S(2)}) copy-start(bf16[256,1408]{1,0:T(8,128)(2,1)} %param.19) | copy-start | bytes 2162692
  28.4 232.7 %all-gather.3.cloned.1.call-start = ((), (), s32[]{:S(2)}) async-start(), calls=%async_computation.2 | async-start | bytes 6488064 | tf_op jit(solution)/shard_map/all_gather | solution.py:96
  28.9 262.3 %all-gather.5.cloned.1.call-start = ((), (), s32[]{:S(2)}) async-start(), calls=%async_computation.3 | async-start | bytes 6488064 | tf_op jit(solution)/shard_map/all_gather | solution.py:97
  29.0 25.9 %collective-permute-start.1 = (bf16[256,1408]{1,0:T(8,128)(2,1)S(1)}, bf16[256,1408]{1,0:T(8,128)(2,1)S(1)}, u32[]{:S(2)}, u32[]{:S(2)}) collective-permute-start(bf16[256,1408]{1,0:T(8,128)(2,1)S(1)} %copy-done.2), channel_id=1, source_target_pairs={{0,4},{4,8},{8,12},{12,16},{16,20},{20,24},{24,28},{28,0},{1,5},{5... | collective-permute-start | bytes 2162696 | tf_op jit(solution)/shard_map/ppermute | solution.py:103
  54.9 33.2 %collective-permute-start.2 = (bf16[256,1408]{1,0:T(8,128)(2,1)S(1)}, bf16[256,1408]{1,0:T(8,128)(2,1)S(1)}, u32[]{:S(2)}, u32[]{:S(2)}) collective-permute-start(bf16[256,1408]{1,0:T(8,128)(2,1)S(1)} %collective-permute-done.1), channel_id=1, source_target_pairs={{0,4},{4,8},{8,12},{12,16},{16,20},{20,24},{24,28},{28,0},{1,5},{5... | collective-permute-start | bytes 2162696 | tf_op jit(solution)/shard_map/ppermute | solution.py:103
  55.8 299.6 %reduce-scatter.2.cloned.1.call-start = ((), (), s32[]{:S(2)}) async-start(), calls=%async_computation.4 | async-start | bytes 5242880 | tf_op jit(solution)/shard_map/reduce_scatter | solution.py:107
  88.1 35.0 %collective-permute-start.3 = (bf16[256,1408]{1,0:T(8,128)(2,1)S(1)}, bf16[256,1408]{1,0:T(8,128)(2,1)S(1)}, u32[]{:S(2)}, u32[]{:S(2)}) collective-permute-start(bf16[256,1408]{1,0:T(8,128)(2,1)S(1)} %collective-permute-done.2), channel_id=1, source_target_pairs={{0,4},{4,8},{8,12},{12,16},{16,20},{20,24},{24,28},{28,0},{1,5},{5... | collective-permute-start | bytes 2162696 | tf_op jit(solution)/shard_map/ppermute | solution.py:103
  123.0 35.1 %collective-permute-start.4 = (bf16[256,1408]{1,0:T(8,128)(2,1)S(1)}, bf16[256,1408]{1,0:T(8,128)(2,1)S(1)}, u32[]{:S(2)}, u32[]{:S(2)}) collective-permute-start(bf16[256,1408]{1,0:T(8,128)(2,1)S(1)} %collective-permute-done.3), channel_id=1, source_target_pairs={{0,4},{4,8},{8,12},{12,16},{16,20},{20,24},{24,28},{28,0},{1,5},{5... | collective-permute-start | bytes 2162696 | tf_op jit(solution)/shard_map/ppermute | solution.py:103
  158.1 0.9 copy-start.3
  159.0 24.7 %collective-permute-start.5 = (bf16[256,1408]{1,0:T(8,128)(2,1)S(1)}, bf16[256,1408]{1,0:T(8,128)(2,1)}, u32[]{:S(2)}, u32[]{:S(2)}) collective-permute-start(bf16[256,1408]{1,0:T(8,128)(2,1)S(1)} %collective-permute-done.4), channel_id=1, source_target_pairs={{0,4},{4,8},{8,12},{12,16},{16,20},{20,24},{24,28},{28,0},{1,5},{5... | collective-permute-start | bytes 2162696 | tf_op jit(solution)/shard_map/ppermute | solution.py:103
  183.7 32.8 %collective-permute-start.6 = (bf16[256,1408]{1,0:T(8,128)(2,1)}, bf16[256,1408]{1,0:T(8,128)(2,1)}, u32[]{:S(2)}, u32[]{:S(2)}) collective-permute-start(bf16[256,1408]{1,0:T(8,128)(2,1)} %collective-permute-done.5), channel_id=1, source_target_pairs={{0,4},{4,8},{8,12},{12,16},{16,20},{20,24},{24,28},{28,0},{1,5},{5... | collective-permute-start | bytes 2162696 | tf_op jit(solution)/shard_map/ppermute | solution.py:103
  216.5 23.0 %collective-permute-start.7 = (bf16[256,1408]{1,0:T(8,128)(2,1)}, bf16[256,1408]{1,0:T(8,128)(2,1)}, u32[]{:S(2)}, u32[]{:S(2)}) collective-permute-start(bf16[256,1408]{1,0:T(8,128)(2,1)} %collective-permute-done.6), channel_id=1, source_target_pairs={{0,4},{4,8},{8,12},{12,16},{16,20},{20,24},{24,28},{28,0},{1,5},{5... | collective-permute-start | bytes 2162696 | tf_op jit(solution)/shard_map/ppermute | solution.py:103
  216.5 29.1 %copy-start.4 = (bf16[256,1408]{1,0:T(8,128)(2,1)S(1)}, bf16[256,1408]{1,0:T(8,128)(2,1)}, u32[]{:S(2)}) copy-start(bf16[256,1408]{1,0:T(8,128)(2,1)} %copy-done.3) | copy-start | bytes 2162692
  250.3 10.8 %copy-start.5 = (f32[2048]{0:T(1024)S(1)}, f32[2048]{0:T(1024)}, u32[]{:S(2)}) copy-start(f32[2048]{0:T(1024)} %param.16) | copy-start | bytes 24580
  291.3 67.0 %copy-start.1 = (bf16[256,2048]{1,0:T(8,128)(2,1)S(1)}, bf16[256,2048]{1,0:T(8,128)(2,1)}, u32[]{:S(2)}) copy-start(bf16[256,2048]{1,0:T(8,128)(2,1)} %param.15) | copy-start | bytes 3145732
Sparse Core Ops, SparseCore 0:
  28.5 85.7 all-reduce.1
  312.4 42.9 reduce-scatter.1
Sparse Core Ops, SparseCore 1:
  31.0 136.0 all-gather.2
  169.2 122.1 all-gather.4
